TPU v7x, 128 devices: a whole 4x4x4 slice. The times are simulated.
128 devices in a mesh: sp: 32 (over z, y, core), tp: 4 (over x).
Axes of the slice: x: 4, y: 4, z: 4, core: 2. Of those that a mesh axis runs over, the one named last changes fastest.
Arguments:
- queries: bfloat16 [16384, 2048], P('sp', 'tp'), may hold values from -6 to 6
- keys: bfloat16 [16384, 512], P('sp', 'tp'), may hold values from -6 to 6
- values: bfloat16 [16384, 512], P('sp', 'tp'), may hold values from -6 to 6
- residual: bfloat16 [16384, 2048], P(('sp', 'tp')), may hold values from -0.119628906 to 0.119628906
- out_proj: bfloat16 [2048, 2048], replicated, may hold values from -0.125 to 0.125
- query_gain: float32 [128], replicated, may hold values from 0.7 to 7
- key_gain: float32 [128], replicated, may hold values from 0.7 to 7
- norm_gain: float32 [2048], replicated, may hold values from 0.1 to 1.9
- routes: int32 [16384, 4], P(('sp', 'tp')), may hold values from 0 to 127, all different within a row; in each aligned block of 128 rows (0 to 127, 128 to 255, ...) at most 8 rows name the same one
- route_weight: float32 [16384, 4], P(('sp', 'tp')), may hold values from 0.1 to 1
- expert_gate: bfloat16 [128, 2048, 256], P(('sp', 'tp')), may hold values from -0.125 to 0.125
- expert_up: bfloat16 [128, 2048, 256], P(('sp', 'tp')), may hold values from -0.125 to 0.125
- expert_down: bfloat16 [128, 256, 2048], P(('sp', 'tp')), may hold values from -0.375 to 0.375
- shared_gate: bfloat16 [2048, 256], replicated, may hold values from -0.125 to 0.125
- shared_up: bfloat16 [2048, 256], replicated, may hold values from -0.125 to 0.125
- shared_down: bfloat16 [256, 2048], replicated, may hold values from -0.375 to 0.375
Outputs:
- layer_out: bfloat16 [16384, 2048], P(('sp', 'tp'))
Inputs may be any that keep to these rules, and one draw needn't show every extreme that they name: In the rows of one device (aligned blocks of 128 tokens), no expert is named by more than 8 routes; some expert is named by exactly 8 routes of some device; the 4 experts of a token differ.
All inputs are finite; a program needn't handle non-finite values.
Results may differ from a plain program's by a relative error of at most 0.023.
The roundings to bfloat16 on the way count: a program that leaves them out, or rounds other values in their place, can miss the bound.
Values may be sent and summed in bfloat16 or wider, within the bound.
No kernel may reach another device: no remote copies, remote signals or barrier semaphores. Data moves between devices by JAX's collectives and lax.ppermute only.
A program may use at most 128 MiB of HBM per device.

v0:
```python
import math

import jax
import jax.numpy as jnp
from jax import lax
from jax.sharding import PartitionSpec as P

HEADS = 16
KV_HEADS = 4
GRID_W = 64


EPS = 1e-06
THETA = 10000.0


def side_by_side(arrays, axis, dim, along):
    both = jnp.concatenate(arrays, axis=along)
    result, at, outs = (lax.all_gather(both, axis, axis=dim, tiled=True), 0, [])
    for a in arrays:
        outs.append(lax.slice_in_dim(result, at, at + a.shape[along], axis=along))
        at += a.shape[along]
    return tuple(outs)


def rotate_pairs(block, cosine, sine):
    first, second = jnp.split(block, 2, axis=-1)
    return jnp.concatenate(
        [first * cosine - second * sine, second * cosine + first * sine], axis=-1
    )


def normed_rotary(source, gain, heads, offset):
    count = source.shape[0]
    width = gain.shape[0]
    values_f = source.astype(jnp.float32).reshape(count, heads, width)
    values_f = (
        values_f * lax.rsqrt(jnp.mean(values_f * values_f, axis=-1, keepdims=True) + EPS) * gain
    )
    position = offset + jnp.arange(count, dtype=jnp.int32)
    grid_row = (position // GRID_W).astype(jnp.float32)
    grid_col = (position % GRID_W).astype(jnp.float32)
    quarter = width // 4
    inverse = jnp.power(THETA, -4.0 * jnp.arange(quarter, dtype=jnp.float32) / width)
    row_angle = (grid_row[:, None] * inverse[None, :])[:, None, :]
    col_angle = (grid_col[:, None] * inverse[None, :])[:, None, :]
    row_half, col_half = jnp.split(values_f, 2, axis=-1)
    turned = jnp.concatenate(
        [
            rotate_pairs(row_half, jnp.cos(row_angle), jnp.sin(row_angle)),
            rotate_pairs(col_half, jnp.cos(col_angle), jnp.sin(col_angle)),
        ],
        axis=-1,
    )
    return turned.reshape(count, heads * width).astype(jnp.bfloat16)


def expert_apply(arrived, expert_gate, expert_up, expert_down):
    sources, slots, width = arrived.shape
    local = expert_gate.shape[0]
    grouped = arrived.reshape(sources // local, local, slots, width)
    gate_part = jnp.einsum(
        "sech,ehf->secf", grouped, expert_gate, preferred_element_type=jnp.float32
    )
    up_part = jnp.einsum("sech,ehf->secf", grouped, expert_up, preferred_element_type=jnp.float32)
    hidden_e = (jax.nn.silu(gate_part) * up_part).astype(jnp.bfloat16)
    result = jnp.einsum("secf,efh->sech", hidden_e, expert_down, preferred_element_type=jnp.float32)
    return result.astype(jnp.bfloat16).reshape(sources, slots, width)


def body(
    queries,
    keys,
    values,
    residual,
    out_proj,
    query_gain,
    key_gain,
    norm_gain,
    routes,
    route_weight,
    expert_gate,
    expert_up,
    expert_down,
    shared_gate,
    shared_up,
    shared_down,
):
    tok_local = queries.shape[0]
    width = query_gain.shape[0]
    group = HEADS // KV_HEADS
    kv_local = keys.shape[1] // width
    scale = 1.0 / math.sqrt(width)
    offset = lax.axis_index("sp") * tok_local
    q_rot = normed_rotary(queries, query_gain, kv_local * group, offset)
    k_rot = normed_rotary(keys, key_gain, kv_local, offset)
    query_3d = q_rot.reshape(tok_local, kv_local, group, width).transpose(1, 2, 0, 3)
    query_3d = query_3d.reshape(kv_local, group * tok_local, width)
    start_state = (
        jnp.full((kv_local, group * tok_local), -jnp.inf, jnp.float32),
        jnp.zeros((kv_local, group * tok_local), jnp.float32),
        jnp.zeros((kv_local, group * tok_local, width), jnp.float32),
    )
    key_piece, value_piece = side_by_side((k_rot, values), "sp", 0, 1)
    count = key_piece.shape[0]
    block = math.gcd(count, 512)

    def one_block(index_block, state):
        running_max, running_sum, accum = state
        key_rows = lax.dynamic_slice_in_dim(key_piece, index_block * block, block, 0)
        value_rows = lax.dynamic_slice_in_dim(value_piece, index_block * block, block, 0)
        key_3d = key_rows.reshape(block, kv_local, width)
        value_3d = value_rows.reshape(block, kv_local, width)
        scores = (
            jnp.einsum("gqd,kgd->gqk", query_3d, key_3d, preferred_element_type=jnp.float32) * scale
        )
        new_max = jnp.maximum(running_max, jnp.max(scores, axis=-1))
        weights = jnp.exp(scores - new_max[..., None])
        factor = jnp.exp(running_max - new_max)
        new_sum = running_sum * factor + jnp.sum(weights, axis=-1)
        added = jnp.einsum(
            "gqk,kgd->gqd",
            weights.astype(jnp.bfloat16),
            value_3d,
            preferred_element_type=jnp.float32,
        )
        return (new_max, new_sum, accum * factor[..., None] + added)

    final_max, final_sum, final_acc = lax.fori_loop(0, count // block, one_block, start_state)
    attn_local = (final_acc / final_sum[..., None]).astype(jnp.bfloat16)
    attn_local = attn_local.reshape(kv_local, group, tok_local, width).transpose(2, 0, 1, 3)
    attn_local = attn_local.reshape(tok_local, kv_local * group * width)
    all_heads = lax.all_to_all(attn_local, "tp", split_axis=0, concat_axis=1, tiled=True)
    projected = jnp.dot(all_heads, out_proj, preferred_element_type=jnp.float32)
    hidden1 = (residual.astype(jnp.float32) + projected).astype(jnp.bfloat16)
    hidden_f = hidden1.astype(jnp.float32)
    normed = (
        hidden_f
        * lax.rsqrt(jnp.mean(hidden_f * hidden_f, axis=-1, keepdims=True) + EPS)
        * norm_gain
    ).astype(jnp.bfloat16)
    rows_local = normed.shape[0]
    top_count = routes.shape[1]
    pair_count = rows_local * top_count
    expert_total = expert_gate.shape[0] * lax.axis_size("sp") * lax.axis_size("tp")
    capacity = max(2, 2 * rows_local * top_count // expert_total)
    flat_routes = routes.reshape(pair_count)
    one_hot = (flat_routes[:, None] == jnp.arange(expert_total, dtype=jnp.int32)[None, :]).astype(
        jnp.float32
    )
    lower = (jnp.arange(pair_count)[:, None] >= jnp.arange(pair_count)[None, :]).astype(jnp.float32)
    running_count = jnp.dot(lower, one_hot, precision=lax.Precision.HIGHEST)
    slot_place = (jnp.sum(running_count * one_hot, axis=1) - 1.0).astype(jnp.int32)
    slot_index = flat_routes * capacity + slot_place
    slot_total = expert_total * capacity
    placement = (jnp.arange(slot_total, dtype=jnp.int32)[:, None] == slot_index[None, :]).astype(
        jnp.bfloat16
    )
    placement = jnp.sum(placement.reshape(slot_total, rows_local, top_count), axis=2)
    send_rows = jnp.dot(placement, normed, preferred_element_type=jnp.float32).astype(jnp.bfloat16)
    send_rows = send_rows.reshape(expert_total, capacity, normed.shape[1])
    shared_hidden = (
        jax.nn.silu(jnp.dot(normed, shared_gate, preferred_element_type=jnp.float32))
        * jnp.dot(normed, shared_up, preferred_element_type=jnp.float32)
    ).astype(jnp.bfloat16)
    shared_out = jnp.dot(shared_hidden, shared_down, preferred_element_type=jnp.float32)
    processed = expert_apply(
        lax.all_to_all(send_rows, ("sp", "tp"), split_axis=0, concat_axis=0, tiled=True),
        expert_gate,
        expert_up,
        expert_down,
    )
    returned = lax.all_to_all(processed, ("sp", "tp"), split_axis=0, concat_axis=0, tiled=True)
    returned = returned.reshape(slot_total, normed.shape[1])
    routed = (
        returned[slot_index].reshape(rows_local, top_count, normed.shape[1]).astype(jnp.float32)
    )
    mixed = jnp.einsum("tk,tkd->td", route_weight, routed) + shared_out
    return (hidden_f + mixed).astype(jnp.bfloat16)


def solution(mesh):
    placed = (
        P("sp", "tp"),
        P("sp", "tp"),
        P("sp", "tp"),
        P(("sp", "tp"), None),
        P(),
        P(),
        P(),
        P(),
        P(("sp", "tp"), None),
        P(("sp", "tp"), None),
        P(("sp", "tp"), None, None),
        P(("sp", "tp"), None, None),
        P(("sp", "tp"), None, None),
        P(),
        P(),
        P(),
    )
    return jax.shard_map(
        body, mesh=mesh, in_specs=placed, out_specs=P(("sp", "tp"), None), check_vma=False
    )
```

profile of v0, /device:TPU:1, one launch (start us, length us, event | category | flops | bytes accessed | tf_op | source)
XLA Modules:
  0.0 400.1 jit_solution(8014369260818085573)
XLA Ops:
  20.2 53.3 %all-gather.2.cloned.1.call-done = bf16[16384,256]{0,1:T(8,128)(2,1)} async-done(((bf16[512,256]{0,1:T(8,128)(2,1)}), bf16[16384,256]{0,1:T(8,128)(2,1)}) %all-gather.2.cloned.1.call-update) | async-done | bytes 8388624 | tf_op jit(solution)/shard_map/all_gather | solution.py:19
  73.5 5.8 %fusion.69 = (bf16[16384,128]{0,1:T(8,128)(2,1)}, bf16[16384,128]{0,1:T(8,128)(2,1)}) fusion(bf16[16384,256]{0,1:T(8,128)(2,1)} %all-gather.2.cloned.1.call-done), kind=kLoop, calls=%fused_computation.125 | loop fusion | bytes 16777216 | tf_op jit(solution)/shard_map/slice | solution.py:21
  79.3 146.8 %while.18 = (s32[]{:T(128)}, f32[1,2048]{1,0:T(1,128)S(1)}, f32[1,2048]{1,0:T(1,128)S(1)}, f32[1,2048,128]{2,1,0:T(8,128)S(1)}, bf16[16384,128]{0,1:T(8,128)(2,1...) while((s32[]{:T(128)}, f32[1,2048]{1,0:T(1,128)S(1)}, ...), condition=%wide.region_5.6_spmd.clone, body=%wide.region_2.5_spmd.clone.sunk | while | flops 546056192 | bytes 15597751 | solution.py:129
  81.7 2.1 fusion.92
  86.3 2.1 fusion.92
  90.9 2.1 fusion.92
  104.7 2.1 fusion.92
  118.5 2.1 fusion.92
  150.6 2.1 fusion.92
  164.4 2.1 fusion.92
  178.1 2.1 fusion.92
  191.9 2.1 fusion.92
  205.7 2.1 fusion.92
  227.9 4.2 %all-to-all-start = ((bf16[4,128,512]{2,1,0:T(8,128)(2,1)}), bf16[4,128,512]{2,1,0:T(8,128)(2,1)S(1)}, u32[]{:S(2)}, u32[]{:S(2)}) async-start(bf16[4,128,512]{2,1,0:T(8,128)(2,1)} %all_to_all.20), calls=%async_computation | async-start | bytes 1048576 | tf_op jit(solution)/shard_map/all_to_all | solution.py:133
  232.6 8.8 %all-to-all-done = bf16[4,128,512]{2,1,0:T(8,128)(2,1)S(1)} async-done(((bf16[4,128,512]{2,1,0:T(8,128)(2,1)}), bf16[4,128,512]{2,1,0:T(8,128)(2,1)S(1)}, u32[]{:S(2)}, u32[]{:S(2)}) %all-to-all-start) | async-done | bytes 524320 | tf_op jit(solution)/shard_map/all_to_all | solution.py:133
  241.7 4.8 %multiply_reduce_fusion.1 = (f32[128]{0:T(128)S(1)}, f32[128,2048]{1,0:T(8,128)S(1)}) fusion(bf16[128,2048]{0,1:T(8,128)(2,1)S(1)} %bitcast.102, bf16[2048,2048]{1,0:T(8,128)(2,1)} %param.22, bf16[128,2048]{1,0:T(8,128)(2,1)} %param.21), kind=kOutput, calls=%fused_computation.47 | convolution fusion | flops 1075314560 | bytes 10486272 | tf_op jit(solution)/shard_map/dot_general | solution.py:134
  247.9 59.7 %all_to_all.29 = bf16[128,8,2048]{2,1,0:T(8,128)(2,1)S(1)} all-to-all(bf16[128,8,2048]{2,1,0:T(8,128)(2,1)S(1)} %convert_bitcast_fusion), channel_id=1, replica_groups=mesh['sp'=32,'tp'=4] {'sp','tp'}, dimensions={0} | all-to-all | bytes 8388608 | tf_op jit(solution)/shard_map/all_to_all | solution.py:168
  311.4 4.3 %copy.56 = bf16[128,8,2048]{2,1,0:T(8,128)(2,1)} copy(bf16[128,8,2048]{2,0,1:T(8,128)(2,1)S(1)} %convolution_convert_fusion) | data formatting | bytes 8388608 | tf_op jit(solution)/shard_map/convert_element_type | solution.py:68
  315.7 5.2 %all-to-all-start.2 = ((bf16[128,8,2048]{2,1,0:T(8,128)(2,1)}), bf16[128,8,2048]{2,1,0:T(8,128)(2,1)}, u32[]{:S(2)}, u32[]{:S(2)}) async-start(bf16[128,8,2048]{2,1,0:T(8,128)(2,1)} %copy.56), calls=%async_computation.2 | async-start | bytes 8388608 | tf_op jit(solution)/shard_map/all_to_all | solution.py:173
  321.6 52.5 %all-to-all-done.2 = bf16[128,8,2048]{2,1,0:T(8,128)(2,1)} async-done(((bf16[128,8,2048]{2,1,0:T(8,128)(2,1)}), bf16[128,8,2048]{2,1,0:T(8,128)(2,1)}, u32[]{:S(2)}, u32[]{:S(2)}) %all-to-all-start.2) | async-done | bytes 4194336 | tf_op jit(solution)/shard_map/all_to_all | solution.py:173
  374.0 8.0 %gather_fusion = bf16[512,2048]{1,0:T(8,128)(2,1)} fusion(bf16[1024,2048]{1,0:T(8,128)(2,1)} %bitcast.29, s32[1024]{0:T(1024)S(1)} %pad_clamp_fusion), kind=kCustom, calls=%fused_computation | custom fusion | bytes 4196352 | tf_op jit(solution)/shard_map/gather | solution.py:176
  382.0 4.2 %reshape.478 = bf16[128,4,2048]{2,1,0:T(4,128)(2,1)} reshape(bf16[512,2048]{1,0:T(8,128)(2,1)} %gather_fusion) | data formatting | bytes 4194304 | tf_op jit(solution)/shard_map/reshape | solution.py:176
  386.2 3.8 fusion.70
  390.0 3.3 fusion.19
  (243 shorter events, 145.7 us)
Async XLA Ops:
  6.5 303.6 %copy-start = (bf16[1,256,2048]{2,1,0:T(8,128)(2,1)S(1)}, bf16[1,256,2048]{2,1,0:T(8,128)(2,1)}, u32[]{:S(2)}) copy-start(bf16[1,256,2048]{2,1,0:T(8,128)(2,1)} %param.30) | copy-start | bytes 3145732
  6.5 9.2 %copy-start.5 = (f32[128]{0:T(128)S(1)}, f32[128]{0:T(128)}, u32[]{:S(2)}) copy-start(f32[128]{0:T(128)} %param.23) | copy-start | bytes 1540
  6.5 67.0 %all-gather.2.cloned.1.call-start = ((), (), s32[]{:S(2)}) async-start(), calls=%async_computation.3 | async-start | bytes 8650752 | tf_op jit(solution)/shard_map/all_gather | solution.py:19
  227.9 13.5 %all-to-all-start = ((bf16[4,128,512]{2,1,0:T(8,128)(2,1)}), bf16[4,128,512]{2,1,0:T(8,128)(2,1)S(1)}, u32[]{:S(2)}, u32[]{:S(2)}) async-start(bf16[4,128,512]{2,1,0:T(8,128)(2,1)} %all_to_all.20), calls=%async_computation | async-start | bytes 1048576 | tf_op jit(solution)/shard_map/all_to_all | solution.py:133
  241.7 4.8 %copy-start.3 = (f32[2048]{0:T(1024)S(1)}, f32[2048]{0:T(1024)}, u32[]{:S(2)}) copy-start(f32[2048]{0:T(1024)} %param.25) | copy-start | bytes 24580
  247.9 59.7 %copy-start.6 = (bf16[1,2048,256]{2,1,0:T(8,128)(2,1)S(1)}, bf16[1,2048,256]{2,1,0:T(8,128)(2,1)}, u32[]{:S(2)}) copy-start(bf16[1,2048,256]{2,1,0:T(8,128)(2,1)} %param.28) | copy-start | bytes 3145732
  307.6 1.3 copy-start.7
  315.7 5.3 %copy-start.4 = (f32[128,4]{0,1:T(4,128)S(1)}, f32[128,4]{0,1:T(4,128)}, u32[]{:S(2)}) copy-start(f32[128,4]{0,1:T(4,128)} %param.27) | copy-start | bytes 6148
  315.7 5.5 %copy-start.2 = (bf16[2048,256]{1,0:T(8,128)(2,1)S(1)}, bf16[2048,256]{1,0:T(8,128)(2,1)}, u32[]{:S(2)}) copy-start(bf16[2048,256]{1,0:T(8,128)(2,1)} %param.31) | copy-start | bytes 3145732
  315.7 58.3 %all-to-all-start.2 = ((bf16[128,8,2048]{2,1,0:T(8,128)(2,1)}), bf16[128,8,2048]{2,1,0:T(8,128)(2,1)}, u32[]{:S(2)}, u32[]{:S(2)}) async-start(bf16[128,8,2048]{2,1,0:T(8,128)(2,1)} %copy.56), calls=%async_computation.2 | async-start | bytes 8388608 | tf_op jit(solution)/shard_map/all_to_all | solution.py:173
  382.0 8.0 %copy-start.1 = (bf16[256,2048]{1,0:T(8,128)(2,1)S(1)}, bf16[256,2048]{1,0:T(8,128)(2,1)}, u32[]{:S(2)}) copy-start(bf16[256,2048]{1,0:T(8,128)(2,1)} %param.33) | copy-start | bytes 3145732
Sparse Core Ops, SparseCore 0:
  10.9 62.5 all-gather.1
where the time goes:
time: 402 us; the launch traced here: 400 us
  matrix products  138 us (34%)
  waiting for transfers between devices  115 us (29%)
  blocking collectives  59.7 us (15%)
  other arithmetic  33.8 us (8%)
  local copies, waits for them, and re-layouts  28.9 us (7%)
  between operations  13.7 us (3%)
  starting transfers between devices  9.41 us (2%)
    dot_general x32, matrix products, one_block(): jnp.einsum('gqk,kgd->gqd', weights.astype(jnp.bfloat16), value_3d, prefer...  67.9 us
    all_to_all x1, blocking collectives, body(): lax.all_to_all(send_rows, ('sp', 'tp'), split_axis=0, concat_axis=0, tile...  59.7 us
    all_gather x1, waiting for transfers between devices, side_by_side(): result, at, outs = (lax.all_gather(both, axis, axis=dim, tiled=True), 0, [])  53.3 us
    dot_general x32, matrix products, one_block(): jnp.einsum('gqd,kgd->gqk', query_3d, key_3d, preferred_element_type=jnp.f...  52.7 us
    all_to_all x1, waiting for transfers between devices, body(): lax.all_to_all(processed, ('sp', 'tp'), split_axis=0, concat_axis=0, tile...  52.5 us
    reduce_sum x32, other arithmetic, one_block(): new_sum = running_sum * factor + jnp.sum(weights, axis=-1)  22.7 us
    all_to_all x1, waiting for transfers between devices, body(): lax.all_to_all(attn_local, 'tp', split_axis=0, concat_axis=1, tiled=True)  8.83 us
  transfers between devices with their start and end apart: 3, of which 3 were waited for; matrix products, arithmetic and copies ran while one was open for 3% of the time, Pallas kernels for 0%

commit v1 on v0

v1 whole, which is shorter than its diff:
```python
import functools
import math

import jax
import jax.numpy as jnp
import numpy as np
from jax import lax
from jax.experimental import pallas as pl
from jax.experimental.pallas import tpu as pltpu
from jax.sharding import Mesh
from jax.sharding import PartitionSpec as P

HEADS = 16
KV_HEADS = 4
GRID_W = 64
HD = 128
CAP = 8
EPS = 1e-06
THETA = 10000.0
LOG2E = math.log2(math.e)
SAFE = 80.0
CHUNKS = 4
VM = pltpu.VMEM


def vspec():
    return pl.BlockSpec(memory_space=VM)


def rotary_tables():
    quarter = HD // 4
    inverse = np.power(THETA, -4.0 * np.arange(quarter, dtype=np.float64) / HD).astype(np.float32)
    angles = (np.arange(256, dtype=np.float32)[:, None] * inverse[None, :]).astype(np.float64)
    cos, sin = np.cos(angles), np.sin(angles)
    cosine = np.concatenate([cos, cos, cos, cos], axis=1).astype(np.float32)
    sine = np.concatenate([-sin, sin, -sin, sin], axis=1).astype(np.float32)
    return cosine, sine


def turned(x, gain, cosine, sine):
    x = x * lax.rsqrt(jnp.mean(x * x, axis=-1, keepdims=True) + EPS) * gain
    lane = lax.broadcasted_iota(jnp.int32, x.shape, 1)
    partner = jnp.where((lane // 32) % 2 == 0, pltpu.roll(x, 96, 1), pltpu.roll(x, 32, 1))
    return x * cosine + partner * sine


def table_pair(row_cos, row_sin, col_cos, col_sin, row):
    lane = lax.broadcasted_iota(jnp.int32, (GRID_W, HD), 1)
    cosine = jnp.where(lane < 64, row_cos[pl.ds(row, 1), :], col_cos[0:GRID_W, :])
    sine = jnp.where(lane < 64, row_sin[pl.ds(row, 1), :], col_sin[0:GRID_W, :])
    return cosine, sine


def kv_prep_kernel(key_ref, value_ref, gain_ref, cos_ref, sin_ref, *out_refs):
    tokens = key_ref.shape[0]
    first_row = lax.axis_index("sp") * (tokens // GRID_W)
    gain = gain_ref[...]
    for c, out_ref in enumerate(out_refs):
        for half in range(2):
            block = 2 * c + half
            cosine, sine = table_pair(cos_ref, sin_ref, cos_ref, sin_ref, first_row + block)
            x = key_ref[GRID_W * block : GRID_W * (block + 1), :].astype(jnp.float32)
            out_ref[GRID_W * half : GRID_W * (half + 1), :] = turned(x, gain, cosine, sine).astype(
                jnp.bfloat16
            )
        v = value_ref[HD * c : HD * (c + 1), :].astype(jnp.float32)
        out_ref[HD : 2 * HD, :] = v.T.astype(jnp.bfloat16)


def q_prep_kernel(query_ref, gain_ref, cos_ref, sin_ref, out_ref):
    tokens = query_ref.shape[0]
    group = query_ref.shape[1] // HD
    first_row = lax.axis_index("sp") * (tokens // GRID_W)
    gain = gain_ref[...]
    factor = LOG2E / math.sqrt(HD)
    for pair in range(tokens // HD):
        tables = [
            table_pair(cos_ref, sin_ref, cos_ref, sin_ref, first_row + 2 * pair + half)
            for half in range(2)
        ]
        for head in range(group):
            parts = []
            for half in range(2):
                at = HD * pair + GRID_W * half
                x = query_ref[at : at + GRID_W, HD * head : HD * (head + 1)].astype(jnp.float32)
                r = turned(x, gain, *tables[half])
                parts.append(r.astype(jnp.bfloat16).astype(jnp.float32))
            flat = jnp.concatenate(parts, axis=0).T * factor
            high = flat.astype(jnp.bfloat16)
            low = (flat - high.astype(jnp.float32)).astype(jnp.bfloat16)
            column = head * tokens + HD * pair
            out_ref[0:HD, column : column + HD] = high
            out_ref[HD : 2 * HD, column : column + HD] = low


def attention_kernel(
    first, last, qt_ref, kv_ref, qg_ref, kg_ref, *rest
):
    if first:
        state_in = None
        outs = rest
    else:
        state_in = rest[:3]
        outs = rest[3:]
    rows = 64
    blocks = kv_ref.shape[0]
    tiles = blocks // 2
    columns = qt_ref.shape[1]
    if last:
        final_ref, acc_ref, sum_ref, max_ref = outs
    else:
        acc_ref, sum_ref, max_ref = outs
    bound = jnp.max(jnp.abs(qg_ref[...])) * jnp.max(jnp.abs(kg_ref[...]))
    bound = bound * (1.02 * LOG2E * math.sqrt(HD))
    safe = bound <= SAFE

    def scoped(*accs):
        scores = [[[accs[(b * 2 + m) * 4 + r] for r in range(4)] for m in range(2)] for b in range(3)]
        total = [accs[24 + m] for m in range(2)]

        def query_key(tile, slot, base):
            for m in range(2):
                pltpu.matmul_push_rhs(
                    qt_ref[:, pl.ds(base + 256 * m, 256)], staging_register=0, mxu_index=m
                )
            for r in range(4):
                k = kv_ref[2 * tile + r // 2, (r % 2) * rows : (r % 2 + 1) * rows, :]
                kk = jnp.concatenate([k, k], axis=1)
                for m in range(2):
                    pltpu.matmul_acc_lhs(
                        scores[slot][m][r], kk, load_staged_rhs=0 if r == 0 else None
                    )

        def weigh_values(tile, slot, sums, shifts):
            sums = list(sums)
            for m in range(2):
                pieces = []
                for r in range(4):
                    s = pltpu.matmul_pop(scores[slot][m][r])
                    if shifts is not None:
                        s = s - shifts[m]
                    e = jnp.exp2(s)
                    sums[m] = sums[m] + jnp.sum(e.reshape(rows // 8, 8, 256), axis=0)
                    pieces.append(e.astype(jnp.bfloat16))
                pltpu.matmul_push_rhs(
                    jnp.concatenate(pieces, axis=0), staging_register=1, mxu_index=m
                )
            v = jnp.concatenate(
                [kv_ref[2 * tile, HD : 2 * HD, :], kv_ref[2 * tile + 1, HD : 2 * HD, :]], axis=1
            )
            for m in range(2):
                pltpu.matmul_acc_lhs(total[m], v, load_staged_rhs=1)
            return tuple(sums)

        zero_sums = tuple(jnp.zeros((8, 256), jnp.float32) for _ in range(2))

        @pl.when(safe)
        def _():
            def trip(j, carry):
                base = pl.multiple_of(j * 512, 512)
                query_key(0, 0, base)
                query_key(1, 1, base)
                sums = zero_sums
                for t in range(tiles):
                    if t + 2 < tiles:
                        query_key(t + 2, (t + 2) % 3, base)
                    sums = weigh_values(t, t % 3, sums, None)
                for m in range(2):
                    at = pl.ds(base + 256 * m, 256)
                    added = pltpu.matmul_pop(total[m])
                    if state_in is None:
                        acc_ref[:, at] = added
                        sum_ref[:, at] = sums[m]
                        max_ref[:, at] = jnp.zeros((8, 256), jnp.float32)
                    else:
                        acc_ref[:, at] = state_in[0][:, at] + added
                        sum_ref[:, at] = state_in[1][:, at] + sums[m]
                        max_ref[:, at] = state_in[2][:, at]
                return carry

            lax.fori_loop(0, columns // 512, trip, 0)

        @pl.when(jnp.logical_not(safe))
        def _():
            def trip(j, carry):
                base = pl.multiple_of(j * 512, 512)
                spans = [pl.ds(base + 256 * m, 256) for m in range(2)]

                def largest(t, tops):
                    query_key(t, 0, base)
                    new = []
                    for m in range(2):
                        top = tops[m]
                        for r in range(4):
                            s = pltpu.matmul_pop(scores[0][m][r])
                            top = jnp.maximum(top, jnp.max(s.reshape(rows // 8, 8, 256), axis=0))
                        new.append(top)
                    return tuple(new)

                if state_in is None:
                    old = tuple(jnp.full((8, 256), -1e30, jnp.float32) for _ in range(2))
                else:
                    old = tuple(state_in[2][:, at] for at in spans)
                tops = lax.fori_loop(0, tiles, largest, old)
                tops = [
                    jnp.broadcast_to(jnp.max(top, axis=0, keepdims=True), (8, 256)) for top in tops
                ]
                shifts = [top[0:1, :] for top in tops]

                def weigh(t, sums):
                    query_key(t, 0, base)
                    return weigh_values(t, 0, sums, shifts)

                sums = lax.fori_loop(0, tiles, weigh, zero_sums)
                for m, at in enumerate(spans):
                    added = pltpu.matmul_pop(total[m])
                    max_ref[:, at] = tops[m]
                    if state_in is None:
                        acc_ref[:, at] = added
                        sum_ref[:, at] = sums[m]
                    else:
                        factor = jnp.exp2(old[m] - tops[m])
                        acc_ref[:, at] = state_in[0][:, at] * factor[0:1, :] + added
                        sum_ref[:, at] = state_in[1][:, at] * factor + sums[m]
                return carry

            lax.fori_loop(0, columns // 512, trip, 0)

    specs = [pltpu.ACC(m)((rows, 256), jnp.float32) for _ in range(3) for m in range(2) for _ in range(4)]
    specs += [pltpu.ACC(m)((HD, 256), jnp.float32) for m in range(2)]
    pl.run_scoped(scoped, *specs)

    if last:
        tokens = final_ref.shape[0]

        def finish(i, carry):
            for head in range(columns // tokens):
                at = pl.ds(pl.multiple_of(head * tokens + i * HD, HD), HD)
                denom = jnp.sum(sum_ref[:, at], axis=0, keepdims=True)
                block = acc_ref[:, at] / denom
                final_ref[pl.ds(pl.multiple_of(i * HD, HD), HD), head * HD : (head + 1) * HD] = (
                    block.T.astype(jnp.bfloat16)
                )
            return carry

        lax.fori_loop(0, tokens // HD, finish, 0)


def attention_chunk(qt, kv, query_gain, key_gain, state, last, tokens):
    columns = qt.shape[1]
    first = state is None
    state_shapes = [
        jax.ShapeDtypeStruct((HD, columns), jnp.float32),
        jax.ShapeDtypeStruct((8, columns), jnp.float32),
        jax.ShapeDtypeStruct((8, columns), jnp.float32),
    ]
    keys = kv.shape[0] * HD
    flops = 4 * columns * keys * HD
    args = [qt, kv, query_gain, key_gain] + ([] if first else list(state))
    common = dict(
        in_specs=[vspec()] * len(args),
        compiler_params=pltpu.CompilerParams(vmem_limit_bytes=24 << 20),
        cost_estimate=pl.CostEstimate(flops=4 * flops, bytes_accessed=kv.size * 2, transcendentals=0),
        name="attention",
    )
    kernel = functools.partial(attention_kernel, first, last)
    if last:
        return pl.pallas_call(
            kernel,
            out_shape=jax.ShapeDtypeStruct((tokens, columns // tokens * HD), jnp.bfloat16),
            out_specs=vspec(),
            scratch_shapes=[VM(s.shape, s.dtype) for s in state_shapes],
            **common,
        )(*args)
    return pl.pallas_call(
        kernel, out_shape=state_shapes, out_specs=[vspec()] * 3, **common
    )(*args)


def route_kernel(routes_ref, weight_ref, place_ref, high_ref, low_ref):
    rows, top = routes_ref.shape
    experts = place_ref.shape[0] // CAP
    slots = place_ref.shape[0]
    routes = routes_ref[...]
    weight = weight_ref[...]
    expert = lax.broadcasted_iota(jnp.int32, (rows, experts), 1)
    chosen = jnp.zeros((rows, experts), jnp.float32)
    amount = jnp.zeros((rows, experts), jnp.float32)
    for k in range(top):
        hit = routes[:, k : k + 1] == expert
        chosen = jnp.where(hit, 1.0, chosen)
        amount = jnp.where(hit, weight[:, k : k + 1], amount)
    earlier = (
        lax.broadcasted_iota(jnp.int32, (rows, rows), 0)
        > lax.broadcasted_iota(jnp.int32, (rows, rows), 1)
    ).astype(jnp.bfloat16)
    rank = jnp.dot(earlier, chosen.astype(jnp.bfloat16), preferred_element_type=jnp.float32)
    wide = (
        lax.broadcasted_iota(jnp.int32, (experts, slots), 1) // CAP
        == lax.broadcasted_iota(jnp.int32, (experts, slots), 0)
    ).astype(jnp.bfloat16)
    slot = (lax.broadcasted_iota(jnp.int32, (rows, slots), 1) % CAP).astype(jnp.float32)

    def spread(x):
        return jnp.dot(x.astype(jnp.bfloat16), wide, preferred_element_type=jnp.float32)

    mine = (spread(rank) == slot) & (spread(chosen) > 0.5)
    place_ref[...] = mine.astype(jnp.float32).T.astype(jnp.bfloat16)
    high = amount.astype(jnp.bfloat16).astype(jnp.float32)
    high_ref[...] = jnp.where(mine, spread(high), 0.0).astype(jnp.bfloat16)
    low_ref[...] = jnp.where(mine, spread(amount - high), 0.0).astype(jnp.bfloat16)


def project_kernel(heads_ref, weight_ref, residual_ref, gain_ref, place_ref, hidden_ref, normed_ref, send_ref):
    parts = heads_ref.shape[0]
    depth = heads_ref.shape[2]
    total = residual_ref[...].astype(jnp.float32)
    heads = jnp.concatenate([heads_ref[i] for i in range(parts)], axis=1)
    total = total + jnp.dot(heads, weight_ref[...], preferred_element_type=jnp.float32)
    hidden = total.astype(jnp.bfloat16)
    hidden_ref[...] = hidden
    hidden = hidden.astype(jnp.float32)
    normed = (
        hidden
        * lax.rsqrt(jnp.mean(hidden * hidden, axis=-1, keepdims=True) + EPS)
        * gain_ref[...]
    ).astype(jnp.bfloat16)
    normed_ref[...] = normed
    send_ref[...] = jnp.dot(
        place_ref[...], normed, preferred_element_type=jnp.float32
    ).astype(jnp.bfloat16)


def combine_kernel(returned_ref, high_ref, low_ref, hidden_ref, normed_ref, sg_ref, su_ref, sd_ref, out_ref):
    normed = normed_ref[...]
    gate = jnp.dot(normed, sg_ref[...], preferred_element_type=jnp.float32)
    up = jnp.dot(normed, su_ref[...], preferred_element_type=jnp.float32)
    shared = (jax.nn.silu(gate) * up).astype(jnp.bfloat16)
    returned = returned_ref[...]
    total = jnp.dot(shared, sd_ref[...], preferred_element_type=jnp.float32)
    total = total + jnp.dot(high_ref[...], returned, preferred_element_type=jnp.float32)
    total = total + jnp.dot(low_ref[...], returned, preferred_element_type=jnp.float32)
    out_ref[...] = (hidden_ref[...].astype(jnp.float32) + total).astype(jnp.bfloat16)


def body(
    queries,
    keys,
    values,
    residual,
    out_proj,
    query_gain,
    key_gain,
    norm_gain,
    routes,
    route_weight,
    expert_gate,
    expert_up,
    expert_down,
    shared_gate,
    shared_up,
    shared_down,
):
    tokens = queries.shape[0]
    columns = queries.shape[1] // HD * tokens
    rows = residual.shape[0]
    model = residual.shape[1]
    experts = expert_gate.shape[0] * lax.axis_size("sp") * lax.axis_size("tp")
    slots = experts * CAP
    cosine, sine = (jnp.asarray(t) for t in rotary_tables())
    qg, kg = query_gain.reshape(1, HD), key_gain.reshape(1, HD)
    bf16 = jnp.bfloat16
    shape = jax.ShapeDtypeStruct
    pieces = pl.pallas_call(
        kv_prep_kernel,
        out_shape=[shape((2 * HD, HD), bf16)] * CHUNKS,
        in_specs=[vspec()] * 5,
        out_specs=[vspec()] * CHUNKS,
        name="kv_prep",
    )(keys, values, kg, cosine, sine)
    gathered = [lax.all_gather(p, "sp", axis=0, tiled=False) for p in pieces]
    qt = pl.pallas_call(
        q_prep_kernel,
        out_shape=shape((2 * HD, columns), bf16),
        in_specs=[vspec()] * 4,
        out_specs=vspec(),
        name="q_prep",
    )(queries, qg, cosine, sine)
    place, high, low = pl.pallas_call(
        route_kernel,
        out_shape=[shape((slots, rows), bf16), shape((rows, slots), bf16), shape((rows, slots), bf16)],
        in_specs=[vspec()] * 2,
        out_specs=[vspec()] * 3,
        name="route",
    )(routes, route_weight)
    state = None
    for c, kv in enumerate(gathered):
        state = attention_chunk(qt, kv, qg, kg, state, c == CHUNKS - 1, tokens)
    attn_local = state
    parts = tokens // rows
    all_heads = lax.all_to_all(
        attn_local.reshape(parts, rows, attn_local.shape[1]), "tp", split_axis=0, concat_axis=0, tiled=True
    )
    hidden1, normed, send = pl.pallas_call(
        project_kernel,
        out_shape=[shape((rows, model), bf16), shape((rows, model), bf16), shape((slots, model), bf16)],
        in_specs=[vspec()] * 5,
        out_specs=[vspec()] * 3,
        compiler_params=pltpu.CompilerParams(vmem_limit_bytes=40 << 20),
        name="project",
    )(all_heads, out_proj, residual, norm_gain.reshape(1, model), place)
    arrived = lax.all_to_all(
        send.reshape(experts, CAP, model), ("sp", "tp"), split_axis=0, concat_axis=0, tiled=True
    ).reshape(slots, model)
    gate = jnp.dot(arrived, expert_gate[0], preferred_element_type=jnp.float32)
    up = jnp.dot(arrived, expert_up[0], preferred_element_type=jnp.float32)
    hidden_e = (jax.nn.silu(gate) * up).astype(bf16)
    processed = jnp.dot(hidden_e, expert_down[0], preferred_element_type=jnp.float32).astype(bf16)
    returned = lax.all_to_all(
        processed.reshape(experts, CAP, model), ("sp", "tp"), split_axis=0, concat_axis=0, tiled=True
    ).reshape(slots, model)
    return pl.pallas_call(
        combine_kernel,
        out_shape=shape((rows, model), bf16),
        in_specs=[vspec()] * 8,
        out_specs=vspec(),
        compiler_params=pltpu.CompilerParams(vmem_limit_bytes=40 << 20),
        name="combine",
    )(returned, high, low, hidden1, normed, shared_gate, shared_up, shared_down)


def solution(mesh):
    placed = (
        P("sp", "tp"),
        P("sp", "tp"),
        P("sp", "tp"),
        P(("sp", "tp"), None),
        P(),
        P(),
        P(),
        P(),
        P(("sp", "tp"), None),
        P(("sp", "tp"), None),
        P(("sp", "tp"), None, None),
        P(("sp", "tp"), None, None),
        P(("sp", "tp"), None, None),
        P(),
        P(),
        P(),
    )
    return jax.shard_map(
        body, mesh=mesh, in_specs=placed, out_specs=P(("sp", "tp"), None), check_vma=False
    )
```

time: 402 us -> 393 us (0.978)
  Pallas kernels: 0 us -> 158 us
  matrix products: 138 us -> 11.1 us
  blocking collectives: 59.7 us -> 118 us
  waiting for transfers between devices: 115 us -> 68.1 us
  other arithmetic: 33.8 us -> 0 us
  local copies, waits for them, and re-layouts: 28.9 us -> 19.9 us
  starting transfers between devices: 9.41 us -> 4.09 us
    pallas_call x0 -> x9, Pallas kernels: none -> 158 us  [the longest x3 103 us: attention_chunk(): pl.pallas_call(kernel, out_shape=state_shapes, out_specs=[vspec()] * 3, *...]
    dot_general x73 -> x2, matrix products: 138 us -> 11.1 us  [the longest x1 8.85 us: body(): jnp.dot(hidden_e, expert_down[0], preferred_element_type=jnp.float32)]
    all_to_all x1 -> x2, blocking collectives: 59.7 us -> 118 us  [the longest x1 59.7 us: body(): lax.all_to_all(send.reshape(experts, CAP, model), ('sp', 'tp'), split_axi...]
    all_to_all x2 -> x1, waiting for transfers between devices: 61.3 us -> 5.11 us  [body(): lax.all_to_all(attn_local.reshape(parts, rows, attn_local.shape[1]), 'tp'...]
    reduce_sum x35 -> x0, other arithmetic: 23.6 us -> none  [the longest x32 22.7 us: one_block(): new_sum = running_sum * factor + jnp.sum(weights, axis=-1)]
    unnamed x20 -> x62, local copies, waits for them, and re-layouts: 3.08 us -> 19.9 us
    gather x1 -> x0, local copies, waits for them, and re-layouts: 7.99 us -> none  [body(): returned[slot_index].reshape(rows_local, top_count, normed.shape[1])]
    all_gather x1 -> x4, waiting for transfers between devices: 53.3 us -> 61.1 us  [body(): gathered = [lax.all_gather(p, 'sp', axis=0, tiled=False) for p in pieces]]
  transfers between devices with their start and end apart: 3 -> 5, of which waited for: 3 -> 5; matrix products, arithmetic and copies ran while one was open for 3% -> 0% of each run, Pallas kernels for 0% -> 28%
where the time goes in v1:
time: 393 us; the launch traced here: 392 us
  Pallas kernels  158 us (40%)
  blocking collectives  118 us (30%)
  waiting for transfers between devices  68.1 us (17%)
  local copies, waits for them, and re-layouts  19.9 us (5%)
  between operations  13.3 us (3%)
  matrix products  11.1 us (3%)
  starting transfers between devices  4.09 us (1%)
    pallas_call x3, Pallas kernels, attention_chunk(): pl.pallas_call(kernel, out_shape=state_shapes, out_specs=[vspec()] * 3, *...  103 us
    all_gather x4, waiting for transfers between devices, body(): gathered = [lax.all_gather(p, 'sp', axis=0, tiled=False) for p in pieces]  61.1 us
    all_to_all x1, blocking collectives, body(): lax.all_to_all(send.reshape(experts, CAP, model), ('sp', 'tp'), split_axi...  59.7 us
    all_to_all x1, blocking collectives, body(): lax.all_to_all(processed.reshape(experts, CAP, model), ('sp', 'tp'), spli...  58.2 us
    pallas_call x1, Pallas kernels, attention_chunk(): pl.pallas_call(kernel, out_shape=jax.ShapeDtypeStruct((tokens, columns //...  35.6 us
    unnamed x62, local copies, waits for them, and re-layouts  19.9 us
    dot_general x1, matrix products, body(): jnp.dot(hidden_e, expert_down[0], preferred_element_type=jnp.float32)  8.85 us
  transfers between devices with their start and end apart: 5, of which 5 were waited for; matrix products, arithmetic and copies ran while one was open for 0% of the time, Pallas kernels for 28%

profile of v1, /device:TPU:1, one launch (start us, length us, event | category | flops | bytes accessed | tf_op | source)
XLA Modules:
  0.0 392.4 jit_solution(18276715211036593214)
XLA Ops:
  6.5 2.6 kv_prep.1
  11.3 6.1 %q_prep.1.qt_ref = bf16[256,2048]{1,0:T(8,128)(2,1)} custom-call(bf16[512,512]{1,0:T(8,128)(2,1)} %query_ref.1, f32[1,128]{1,0:T(1,128)} %bitcast.42, f32[256,128]{1,0:T(8,128)} %constant.7.clone.cos_ref, f32[256,128]{1,0:T(8,128)} %constant.8.clone.sin_ref), custom_call_target="tpu_custom_call" | custom-call | tf_op jit(solution)/shard_map/q_prep/pallas_call | solution.py:382
  17.4 39.5 %all-gather.15.cloned.1.call-done = bf16[8192,128]{1,0:T(8,128)(2,1)} async-done(((bf16[256,128]{1,0:T(8,128)(2,1)}), bf16[8192,128]{1,0:T(8,128)(2,1)}) %all-gather.15.cloned.1.call-update) | async-done | bytes 2097168 | tf_op jit(solution)/shard_map/all_gather | solution.py:381
  59.5 1.6 copy-done.17
  61.1 34.6 %attention.4 = (f32[128,2048]{1,0:T(8,128)S(1)}, f32[8,2048]{1,0:T(8,128)S(1)}, f32[8,2048]{1,0:T(8,128)S(1)}) custom-call(bf16[256,2048]{1,0:T(8,128)(2,1)S(1)} %copy-done.4, bf16[32,256,128]{2,1,0:T(8,128)(2,1)S(1)} %bitcast.49, f32[1,128]{1,0:T(1,128)S(1)} %bitcast.43, f32[1,128]{1,0:T(1,128)S(1)} %bitcast.38), custom_call_target="tpu_custom_call" | custom-call | flops 17179869184 | bytes 2097152 | tf_op jit(solution)/shard_map/attention/pallas_call | solution.py:275
  96.7 6.1 %all-gather.13.cloned.1.call-done = bf16[8192,128]{1,0:T(8,128)(2,1)} async-done(((bf16[256,128]{1,0:T(8,128)(2,1)}), bf16[8192,128]{1,0:T(8,128)(2,1)}) %all-gather.13.cloned.1.call-update) | async-done | bytes 2097168 | tf_op jit(solution)/shard_map/all_gather | solution.py:381
  102.8 1.6 copy-done.18
  105.6 34.1 %attention.5 = (f32[128,2048]{1,0:T(8,128)S(1)}, f32[8,2048]{1,0:T(8,128)S(1)}, f32[8,2048]{1,0:T(8,128)S(1)}) custom-call(bf16[256,2048]{1,0:T(8,128)(2,1)S(1)} %copy-done.5, bf16[32,256,128]{2,1,0:T(8,128)(2,1)S(1)} %bitcast.50, f32[1,128]{1,0:T(1,128)S(1)} %bitcast.44, f32[1,128]{1,0:T(1,128)S(1)} %bitcast.39, f32[128,2048]{1,0:T(8,128)S(1)} %copy-done.24, ...), custom_call_target="tpu_custom_call" | custom-call | flops 17179869184 | bytes 2097152 | tf_op jit(solution)/shard_map/attention/pallas_call | solution.py:275
  140.7 8.0 %all-gather.11.cloned.1.call-done = bf16[8192,128]{1,0:T(8,128)(2,1)} async-done(((bf16[256,128]{1,0:T(8,128)(2,1)}), bf16[8192,128]{1,0:T(8,128)(2,1)}) %all-gather.11.cloned.1.call-update) | async-done | bytes 2097168 | tf_op jit(solution)/shard_map/all_gather | solution.py:381
  148.7 1.6 copy-done.15
  151.5 34.1 %attention.6 = (f32[128,2048]{1,0:T(8,128)S(1)}, f32[8,2048]{1,0:T(8,128)S(1)}, f32[8,2048]{1,0:T(8,128)S(1)}) custom-call(bf16[256,2048]{1,0:T(8,128)(2,1)S(1)} %copy-done.5, bf16[32,256,128]{2,1,0:T(8,128)(2,1)S(1)} %bitcast.47, f32[1,128]{1,0:T(1,128)S(1)} %bitcast.45, f32[1,128]{1,0:T(1,128)S(1)} %bitcast.40, f32[128,2048]{1,0:T(8,128)S(1)} %copy-done.22, ...), custom_call_target="tpu_custom_call" | custom-call | flops 17179869184 | bytes 2097152 | tf_op jit(solution)/shard_map/attention/pallas_call | solution.py:275
  186.6 7.4 %all-gather.9.cloned.1.call-done = bf16[8192,128]{1,0:T(8,128)(2,1)} async-done(((bf16[256,128]{1,0:T(8,128)(2,1)}), bf16[8192,128]{1,0:T(8,128)(2,1)}) %all-gather.9.cloned.1.call-update) | async-done | bytes 2097168 | tf_op jit(solution)/shard_map/all_gather | solution.py:381
  194.1 1.6 copy-done.16
  196.9 35.6 %attention.7 = bf16[512,512]{1,0:T(8,128)(2,1)} custom-call(bf16[256,2048]{1,0:T(8,128)(2,1)S(1)} %copy-done.5, bf16[32,256,128]{2,1,0:T(8,128)(2,1)S(1)} %bitcast.48, f32[1,128]{1,0:T(1,128)S(1)} %bitcast.46, f32[1,128]{1,0:T(1,128)S(1)} %bitcast.41, f32[128,2048]{1,0:T(8,128)S(1)} %copy-done.20, f32[8,2048]{1,0:T(8,128)S(1)} %get-tuple-element.35.rest_1_, ...), custom_call_target="tpu_custom_call" | custom-call | flops 17179869184 | bytes 2097152 | tf_op jit(solution)/shard_map/attention/pallas_call | solution.py:268
  232.5 4.0 %all-to-all-start = ((bf16[4,128,512]{2,1,0:T(8,128)(2,1)}), bf16[4,128,512]{2,1,0:T(8,128)(2,1)S(1)}, u32[]{:S(2)}, u32[]{:S(2)}) async-start(bf16[4,128,512]{2,1,0:T(8,128)(2,1)} %bitcast.6), calls=%async_computation | async-start | bytes 1048576 | tf_op jit(solution)/shard_map/all_to_all | solution.py:401
  237.9 2.4 route.1
  240.3 5.1 %all-to-all-done.heads_ref = bf16[4,128,512]{2,1,0:T(8,128)(2,1)S(1)} async-done(((bf16[4,128,512]{2,1,0:T(8,128)(2,1)}), bf16[4,128,512]{2,1,0:T(8,128)(2,1)S(1)}, u32[]{:S(2)}, u32[]{:S(2)}) %all-to-all-start) | async-done | bytes 524320 | tf_op jit(solution)/shard_map/all_to_all | solution.py:401
  246.4 6.1 %project.1 = (bf16[128,2048]{1,0:T(8,128)(2,1)S(1)}, bf16[128,2048]{1,0:T(8,128)(2,1)S(1)}, bf16[1024,2048]{1,0:T(8,128)(2,1)S(1)}) custom-call(bf16[4,128,512]{2,1,0:T(8,128)(2,1)S(1)} %all-to-all-done.heads_ref, bf16[2048,2048]{1,0:T(8,128)(2,1)} %weight_ref.2, bf16[128,2048]{1,0:T(8,128)(2,1)S(1)} %copy-done.6, f32[1,2048]{1,0:T(1,128)S(1)} %bitcast.36, ...), custom_call_target="tpu_custom_call" | custom-call | tf_op jit(solution)/shard_map/project/pallas_call | solution.py:404
  252.5 59.7 %all_to_all.15 = bf16[128,8,2048]{2,1,0:T(8,128)(2,1)S(1)} all-to-all(bf16[128,8,2048]{2,1,0:T(8,128)(2,1)S(1)} %bitcast.35), channel_id=1, replica_groups=mesh['sp'=32,'tp'=4] {'sp','tp'}, dimensions={0} | all-to-all | bytes 8388608 | tf_op jit(solution)/shard_map/all_to_all | solution.py:412
  312.2 2.0 copy-done.25
  314.1 2.2 fusion.2
  316.4 8.8 %convert_bitcast_fusion = bf16[128,8,2048]{2,1,0:T(8,128)(2,1)} fusion(bf16[1,256,2048]{2,1,0:T(8,128)(2,1)S(1)} %copy-done, bf16[128,8,2048]{2,1,0:T(8,128)(2,1)} %copy-done.25, bf16[1,2048,256]{2,1,0:T(8,128)(2,1)S(1)} %copy-done.29, f32[1024,256]{1,0:T(8,128)} %fusion.2), kind=kOutput, calls=%fused_computation.4 | convolution fusion | flops 2151153664 | bytes 11534336 | tf_op jit(solution)/shard_map/dot_general | solution.py:418
  325.2 58.2 %all_to_all.16 = bf16[128,8,2048]{2,1,0:T(8,128)(2,1)S(1)} all-to-all(bf16[128,8,2048]{2,1,0:T(8,128)(2,1)} %convert_bitcast_fusion), channel_id=1, replica_groups=mesh['sp'=32,'tp'=4] {'sp','tp'}, dimensions={0} | all-to-all | bytes 8388608 | tf_op jit(solution)/shard_map/all_to_all | solution.py:419
  383.4 2.5 combine.1
  (65 shorter events, 13.6 us)
Async XLA Ops:
  6.5 309.8 %copy-start = (bf16[1,256,2048]{2,1,0:T(8,128)(2,1)S(1)}, bf16[1,256,2048]{2,1,0:T(8,128)(2,1)}, u32[]{:S(2)}) copy-start(bf16[1,256,2048]{2,1,0:T(8,128)(2,1)} %param.30) | copy-start | bytes 3145732
  6.5 50.4 %all-gather.15.cloned.1.call-start = ((), (), s32[]{:S(2)}) async-start(), calls=%async_computation.6 | async-start | bytes 2162688 | tf_op jit(solution)/shard_map/all_gather | solution.py:381
  9.2 93.6 %all-gather.13.cloned.1.call-start = ((), (), s32[]{:S(2)}) async-start(), calls=%async_computation.5 | async-start | bytes 2162688 | tf_op jit(solution)/shard_map/all_gather | solution.py:381
  10.0 138.8 %all-gather.11.cloned.1.call-start = ((), (), s32[]{:S(2)}) async-start(), calls=%async_computation.4 | async-start | bytes 2162688 | tf_op jit(solution)/shard_map/all_gather | solution.py:381
  10.7 183.4 %all-gather.9.cloned.1.call-start = ((), (), s32[]{:S(2)}) async-start(), calls=%async_computation.3 | async-start | bytes 2162688 | tf_op jit(solution)/shard_map/all_gather | solution.py:381
  59.5 1.6 copy-start.17
  61.1 41.7 %copy-start.5 = (bf16[256,2048]{1,0:T(8,128)(2,1)S(1)}, bf16[256,2048]{1,0:T(8,128)(2,1)}, u32[]{:S(2)}) copy-start(bf16[256,2048]{1,0:T(8,128)(2,1)} %q_prep.1.qt_ref) | copy-start | bytes 3145732
  61.1 41.7 %copy-start.12 = (f32[128]{0:T(128)S(1)}, f32[128]{0:T(128)}, u32[]{:S(2)}) copy-start(f32[128]{0:T(128)} %param.24) | copy-start | bytes 1540
  61.1 41.7 %copy-start.14 = (f32[128]{0:T(128)S(1)}, f32[128]{0:T(128)}, u32[]{:S(2)}) copy-start(f32[128]{0:T(128)} %param.23) | copy-start | bytes 1540
  102.8 1.6 copy-start.18
  148.7 1.6 copy-start.15
  196.9 39.6 %copy-start.26 = (s32[128,4]{0,1:T(4,128)S(1)}, s32[128,4]{0,1:T(4,128)}, u32[]{:S(2)}) copy-start(s32[128,4]{0,1:T(4,128)} %param.26) | copy-start | bytes 6148
  196.9 40.3 %copy-start.27 = (f32[128,4]{0,1:T(4,128)S(1)}, f32[128,4]{0,1:T(4,128)}, u32[]{:S(2)}) copy-start(f32[128,4]{0,1:T(4,128)} %param.27) | copy-start | bytes 6148
  196.9 48.6 %copy-start.6 = (bf16[128,2048]{1,0:T(8,128)(2,1)S(1)}, bf16[128,2048]{1,0:T(8,128)(2,1)}, u32[]{:S(2)}) copy-start(bf16[128,2048]{1,0:T(8,128)(2,1)} %residual_ref.1) | copy-start | bytes 1572868
  196.9 48.6 %copy-start.10 = (f32[2048]{0:T(1024)S(1)}, f32[2048]{0:T(1024)}, u32[]{:S(2)}) copy-start(f32[2048]{0:T(1024)} %param.25) | copy-start | bytes 24580
  232.5 13.0 %all-to-all-start = ((bf16[4,128,512]{2,1,0:T(8,128)(2,1)}), bf16[4,128,512]{2,1,0:T(8,128)(2,1)S(1)}, u32[]{:S(2)}, u32[]{:S(2)}) async-start(bf16[4,128,512]{2,1,0:T(8,128)(2,1)} %bitcast.6), calls=%async_computation | async-start | bytes 1048576 | tf_op jit(solution)/shard_map/all_to_all | solution.py:401
  252.5 61.6 %copy-start.28 = (bf16[1,2048,256]{2,1,0:T(8,128)(2,1)S(1)}, bf16[1,2048,256]{2,1,0:T(8,128)(2,1)}, u32[]{:S(2)}) copy-start(bf16[1,2048,256]{2,1,0:T(8,128)(2,1)} %param.28) | copy-start | bytes 3145732
  312.2 2.0 copy-start.25
  314.1 2.2 copy-start.29
  325.2 58.2 %copy-start.1 = (bf16[2048,256]{1,0:T(8,128)(2,1)S(1)}, bf16[2048,256]{1,0:T(8,128)(2,1)}, u32[]{:S(2)}) copy-start(bf16[2048,256]{1,0:T(8,128)(2,1)} %sg_ref.1) | copy-start | bytes 3145732
  325.2 58.2 %copy-start.2 = (bf16[2048,256]{1,0:T(8,128)(2,1)S(1)}, bf16[2048,256]{1,0:T(8,128)(2,1)}, u32[]{:S(2)}) copy-start(bf16[2048,256]{1,0:T(8,128)(2,1)} %su_ref.1) | copy-start | bytes 3145732
  325.2 58.2 %copy-start.3 = (bf16[256,2048]{1,0:T(8,128)(2,1)S(1)}, bf16[256,2048]{1,0:T(8,128)(2,1)}, u32[]{:S(2)}) copy-start(bf16[256,2048]{1,0:T(8,128)(2,1)} %sd_ref.1) | copy-start | bytes 3145732
  325.2 58.2 %copy-start.7 = (bf16[128,1024]{1,0:T(8,128)(2,1)S(1)}, bf16[128,1024]{1,0:T(8,128)(2,1)}, u32[]{:S(2)}) copy-start(bf16[128,1024]{1,0:T(8,128)(2,1)} %get-tuple-element.39.high_ref) | copy-start | bytes 786436
  325.2 58.2 %copy-start.8 = (bf16[128,1024]{1,0:T(8,128)(2,1)S(1)}, bf16[128,1024]{1,0:T(8,128)(2,1)}, u32[]{:S(2)}) copy-start(bf16[128,1024]{1,0:T(8,128)(2,1)} %get-tuple-element.40.low_ref) | copy-start | bytes 786436
  (11 other events, 11.7 us)
Sparse Core Ops, SparseCore 0:
  9.6 47.3 all-gather.14
  59.2 43.4 all-gather.12
  105.0 43.6 all-gather.10
  150.8 43.1 all-gather.8
